TPU v7x, 32 devices: a whole 2x2x4 slice. The times are simulated.
32 devices in a mesh: tp: 8 (over z, core), dp: 4 (over y, x).
Axes of the slice: x: 2, y: 2, z: 4, core: 2. Of those that a mesh axis runs over, the one named last changes fastest.
Arguments:
- tokens: bfloat16 [32, 4096], P('tp', 'dp'), may hold values from -30 to 30
- lengths: int32 [32], P('dp'), may hold values from 1 to 8192, 65536 in all
- in_gain: float32 [2, 4096], P(None, 'dp'), may hold values from 0.1 to 1.9
- w_recept: bfloat16 [2, 4096, 2048], P(None, 'dp', 'tp'), may hold values from -0.09375 to 0.09375
- w_key: bfloat16 [2, 4096, 2048], P(None, 'dp', 'tp'), may hold values from -0.09375 to 0.09375
- w_value: bfloat16 [2, 4096, 2048], P(None, 'dp', 'tp'), may hold values from -0.09375 to 0.09375
- w_decay: bfloat16 [2, 4096, 2048], P(None, 'dp', 'tp'), may hold values from -0.09375 to 0.09375
- w_rate: bfloat16 [2, 4096, 2048], P(None, 'dp', 'tp'), may hold values from -0.09375 to 0.09375
- w_gate: bfloat16 [2, 4096, 2048], P(None, 'dp', 'tp'), may hold values from -0.09375 to 0.09375
- w_out: bfloat16 [2, 2048, 4096], P(None, 'tp', 'dp'), may hold values from -0.125 to 0.125
- decay_base: float32 [2, 2048], P(None, 'tp'), may hold values from -6 to 6
- mix_gain: float32 [2, 2048], P(None, 'tp'), may hold values from 0.1 to 1.9
- states: float32 [2, 32, 32, 64, 64], P(None, 'dp', 'tp'), may hold values from -6 to 6
Outputs:
- next_tokens: bfloat16 [32, 4096], P('tp', 'dp')
- new_states: float32 [2, 32, 32, 64, 64], P(None, 'dp', 'tp')
All inputs are finite; a program needn't handle non-finite values. No bound on the sum of `lengths` on one device may be relied on, other than what follows from the above.
Results may differ from a plain program's by a relative error of at most 0.0065.
Values may be sent and summed in bfloat16 or wider, within the bound.
A program may use at most 64 MiB of HBM per device.

v0:
```python
import functools

import jax
import jax.numpy as jnp
from jax import lax
from jax.experimental import pallas as pl
from jax.experimental.pallas import tpu as pltpu
from jax.sharding import PartitionSpec as P

POSITION = 2048
DECAY_SCALE = 0.6065306597126334
NORM_EPS = 1e-06
KEY_EPS = 1e-05
GROUP_EPS = 0.00064
ROLES = 6
GROUPS = 3
MESH = pl.DeviceIdType.MESH


def step_kernel(
    tp,
    dp,
    lengths_hbm,
    tokens,
    in_gain,
    decay_base,
    mix_gain,
    w_recept,
    w_key,
    w_value,
    w_decay,
    w_rate,
    w_gate,
    w_out,
    states,
    next_tokens,
    new_states,
    lengths,
    gain_v,
    base_v,
    mixgain_v,
    w_v,
    wo_v,
    s_v,
    xg,
    x32,
    psum,
    rbuf,
    vec,
    rows,
    mg,
    osum,
    obuf,
    small_sem,
    w_sem,
    wo_sem,
    s_sem,
    out_sem,
    ag_s,
    ag_r,
    rs_s,
    rs_r,
    mg_s,
    mg_r,
    os_s,
    os_r,
):
    layers, row_count, heads, size, _ = states.shape
    rt, cl = tokens.shape
    width = heads * size
    batch = rt * tp
    model = cl * dp
    me_tp = lax.axis_index("tp")
    me_dp = lax.axis_index("dp")
    far_first = sorted(range(1, tp), key=lambda k: -min(k, tp - k))
    tp_peers = [lax.rem(me_tp + k, tp) for k in far_first]
    dp_peers = [lax.rem(me_dp + k, dp) for k in range(1, dp)]

    tok_copy = pltpu.make_async_copy(tokens, xg.at[0, me_tp], small_sem.at[0])
    tok_copy.start()
    small = [
        pltpu.make_async_copy(in_gain, gain_v, small_sem.at[1]),
        pltpu.make_async_copy(decay_base, base_v, small_sem.at[2]),
        pltpu.make_async_copy(mix_gain, mixgain_v, small_sem.at[3]),
        pltpu.make_async_copy(lengths_hbm, lengths, small_sem.at[4]),
    ]
    for copy in small:
        copy.start()
    w_copies, wo_copies, s_copies = [], [], []
    for l in range(layers):
        per_role = []
        for r, w in enumerate((w_recept, w_key, w_value, w_decay, w_rate, w_gate)):
            per_role.append(pltpu.make_async_copy(w.at[l], w_v.at[l, r], w_sem.at[l, r]))
        w_copies.append(per_role)
        s_copies.append(pltpu.make_async_copy(states.at[l], s_v.at[l], s_sem.at[l]))
        wo_copies.append(pltpu.make_async_copy(w_out.at[l], wo_v.at[l], wo_sem.at[l]))
        for copy in per_role + [s_copies[l], wo_copies[l]]:
            copy.start()

    barrier = pltpu.get_barrier_semaphore()
    for peer in tp_peers:
        pl.semaphore_signal(barrier, inc=1, device_id={"tp": peer}, device_id_type=MESH)
    for peer in dp_peers:
        pl.semaphore_signal(barrier, inc=1, device_id={"dp": peer}, device_id_type=MESH)
    pl.semaphore_wait(barrier, tp - 1 + dp - 1)

    sends = []

    def exchange(src, dst, send_sem, recv_sem, axis, peer):
        copy = pltpu.make_async_remote_copy(
            src_ref=src,
            dst_ref=dst,
            send_sem=send_sem,
            recv_sem=recv_sem,
            device_id={axis: peer},
            device_id_type=MESH,
        )
        copy.start()
        sends.append(copy)
        return copy

    def gather_tokens(l):
        return [
            exchange(xg.at[l, me_tp], xg.at[l, me_tp], ag_s.at[l, k], ag_r.at[l, k], "tp", peer)
            for k, peer in enumerate(tp_peers)
        ]

    tok_copy.wait()
    incoming = gather_tokens(0)
    for copy in small:
        copy.wait()

    row_at = lax.broadcasted_iota(jnp.int32, (row_count, width), 0)
    len_rows = jnp.zeros((row_count, width), jnp.int32)
    for b in range(row_count):
        len_rows = jnp.where(row_at == b, lengths[b], len_rows)
    live_rows = len_rows > POSITION
    cube = (heads, size, size)
    eye = lax.broadcasted_iota(jnp.int32, cube, 1) == lax.broadcasted_iota(jnp.int32, cube, 2)
    out_copies = []

    for l in range(layers):
        for copy in incoming:
            copy.wait_recv()
        for i in range(tp):
            x32[i * rt : (i + 1) * rt, :] = xg[l, i].astype(jnp.float32)
        x = x32[...]
        squares = jnp.sum(x * x, axis=1, keepdims=True)
        spread_sq = jnp.broadcast_to(squares, (batch, width)).reshape(dp, row_count, width)
        coarse = spread_sq.astype(jnp.bfloat16)
        psum[l, :, 0] = coarse
        psum[l, :, 1] = (spread_sq - coarse.astype(jnp.float32)).astype(jnp.bfloat16)
        scaled = (x * gain_v[l : l + 1, :]).astype(jnp.bfloat16)
        incoming = []
        for r in range(ROLES):
            w_copies[l][r].wait()
            part = jnp.dot(scaled, w_v[l, r], preferred_element_type=jnp.float32)
            psum[l, :, r + 2] = part.reshape(dp, row_count, width).astype(jnp.bfloat16)
            if (r + 1) % (ROLES // GROUPS) == 0:
                g = r // (ROLES // GROUPS)
                lo = 0 if g == 0 else r + 3 - ROLES // GROUPS
                cut = pl.ds(lo, r + 3 - lo)
                for k, peer in enumerate(dp_peers):
                    incoming.append(
                        exchange(
                            psum.at[l, peer, cut],
                            rbuf.at[l, k, cut],
                            rs_s.at[l, g, k],
                            rs_r.at[l, g, k],
                            "dp",
                            peer,
                        )
                    )
        s_copies[l].wait()
        for copy in incoming:
            copy.wait_recv()
        total = []
        for r in range(ROLES + 2):
            plane = psum[l, me_dp, r].astype(jnp.float32)
            for k in range(dp - 1):
                plane = plane + rbuf[l, k, r].astype(jnp.float32)
            total.append(plane)
        inverse = lax.rsqrt((total[0] + total[1]) / model + NORM_EPS)
        recept, key, value, decay_pre, rate_pre, gate_pre = [plane * inverse for plane in total[2:]]
        decay = jnp.exp(-DECAY_SCALE * jax.nn.sigmoid(decay_pre + base_v[l : l + 1, :]))
        rate = jax.nn.sigmoid(rate_pre)
        offsets = []
        for h in range(heads):
            at = slice(h * size, (h + 1) * size)
            key_h, recept_h, decay_h, value_h = key[:, at], recept[:, at], decay[:, at], value[:, at]
            unit = key_h * lax.rsqrt(jnp.sum(key_h * key_h, axis=1, keepdims=True) + KEY_EPS)
            paced = unit * rate[:, at]
            along = jnp.sum(paced * recept_h, axis=1, keepdims=True)
            offsets.append(value_h * jnp.sum(key_h * recept_h, axis=1, keepdims=True))
            vec[0, h] = decay_h * recept_h - along * unit
            vec[1, h] = unit
            vec[2, h] = decay_h
            vec[3, h] = paced
            vec[4, h] = key_h
            vec[5, h] = value_h

        def read_row(b, carry, l=l):
            column = jnp.sum(s_v[l, b] * vec[0, :, pl.ds(b, 1), :], axis=2, keepdims=True)
            rows[:, pl.ds(b, 1), :] = jnp.sum(jnp.where(eye, column, 0.0), axis=1, keepdims=True)
            return carry

        lax.fori_loop(0, row_count, read_row, 0, unroll=True)
        pieces = []
        for h in range(heads):
            readout = rows[h] + offsets[h]
            moved = readout - jnp.mean(readout, axis=1, keepdims=True)
            spread = jnp.mean(moved * moved, axis=1, keepdims=True)
            pieces.append(moved * lax.rsqrt(spread + GROUP_EPS))
        normed = jnp.concatenate(pieces, axis=1) if heads > 1 else pieces[0]
        normed = normed * mixgain_v[l : l + 1, :] * jax.nn.sigmoid(gate_pre)
        mg[l, me_dp] = jnp.where(live_rows, normed, 0.0).astype(jnp.bfloat16)
        incoming = [
            exchange(mg.at[l, me_dp], mg.at[l, me_dp], mg_s.at[l, k], mg_r.at[l, k], "dp", peer)
            for k, peer in enumerate(dp_peers)
        ]

        def renew(b, carry, l=l):
            old = s_v[l, b]
            taken = jnp.sum(old * vec[1, :, pl.ds(b, 1), :], axis=2, keepdims=True)
            value_col = jnp.sum(jnp.where(eye, vec[5, :, pl.ds(b, 1), :], 0.0), axis=2, keepdims=True)
            fresh = (
                old * vec[2, :, pl.ds(b, 1), :]
                - taken * vec[3, :, pl.ds(b, 1), :]
                + value_col * vec[4, :, pl.ds(b, 1), :]
            )
            live = jnp.full(cube, lengths[b], jnp.int32) > POSITION
            s_v[l, b] = jnp.where(live, fresh, old)
            return carry

        lax.fori_loop(0, row_count, renew, 0, unroll=True)
        out_copies.append(pltpu.make_async_copy(s_v.at[l], new_states.at[l], out_sem.at[l]))
        out_copies[l].start()

        wo_copies[l].wait()
        for copy in incoming:
            copy.wait_recv()
        mixed = mg[l].astype(jnp.float32).reshape(batch, width).astype(jnp.bfloat16)
        terms = jnp.dot(mixed, wo_v[l], preferred_element_type=jnp.float32)
        for i in range(tp):
            osum[l, i] = terms[i * rt : (i + 1) * rt].astype(jnp.bfloat16)
        incoming = [
            exchange(osum.at[l, peer], obuf.at[l, k], os_s.at[l, k], os_r.at[l, k], "tp", peer)
            for k, peer in enumerate(tp_peers)
        ]
        branch = osum[l, me_tp].astype(jnp.float32)
        for k, copy in enumerate(incoming):
            copy.wait_recv()
            branch = branch + obuf[l, k].astype(jnp.float32)
        current = (xg[l, me_tp].astype(jnp.float32) + branch).astype(jnp.bfloat16)
        if l + 1 < layers:
            xg[l + 1, me_tp] = current
            incoming = gather_tokens(l + 1)
        else:
            next_tokens[...] = current

    for copy in sends:
        copy.wait_send()
    for copy in out_copies:
        copy.wait()


def on_device(
    tokens,
    lengths,
    in_gain,
    w_recept,
    w_key,
    w_value,
    w_decay,
    w_rate,
    w_gate,
    w_out,
    decay_base,
    mix_gain,
    states,
):
    tp = lax.axis_size("tp")
    dp = lax.axis_size("dp")
    layers, row_count, heads, size, _ = states.shape
    rt, cl = tokens.shape
    width = heads * size
    batch = rt * tp
    f32, bf16 = jnp.float32, jnp.bfloat16
    hbm = pl.BlockSpec(memory_space=pl.ANY)
    dma = pltpu.SemaphoreType.DMA
    return pl.pallas_call(
        functools.partial(step_kernel, tp, dp),
        out_shape=(
            jax.ShapeDtypeStruct(tokens.shape, tokens.dtype),
            jax.ShapeDtypeStruct(states.shape, states.dtype),
        ),
        in_specs=[hbm] * 13,
        out_specs=(pl.BlockSpec(memory_space=pltpu.VMEM), hbm),
        scratch_shapes=[
            pltpu.SMEM(lengths.shape, jnp.int32),
            pltpu.VMEM(in_gain.shape, f32),
            pltpu.VMEM(decay_base.shape, f32),
            pltpu.VMEM(mix_gain.shape, f32),
            pltpu.VMEM((layers, ROLES) + w_key.shape[1:], bf16),
            pltpu.VMEM(w_out.shape, bf16),
            pltpu.VMEM(states.shape, f32),
            pltpu.VMEM((layers, tp, rt, cl), bf16),
            pltpu.VMEM((batch, cl), f32),
            pltpu.VMEM((layers, dp, ROLES + 2, row_count, width), bf16),
            pltpu.VMEM((layers, dp - 1, ROLES + 2, row_count, width), bf16),
            pltpu.VMEM((6, heads, row_count, size), f32),
            pltpu.VMEM((heads, row_count, size), f32),
            pltpu.VMEM((layers, dp, row_count, width), bf16),
            pltpu.VMEM((layers, tp, rt, cl), bf16),
            pltpu.VMEM((layers, tp - 1, rt, cl), bf16),
            dma((5,)),
            dma((layers, ROLES)),
            dma((layers,)),
            dma((layers,)),
            dma((layers,)),
            dma((layers, tp - 1)),
            dma((layers, tp - 1)),
            dma((layers, GROUPS, dp - 1)),
            dma((layers, GROUPS, dp - 1)),
            dma((layers, dp - 1)),
            dma((layers, dp - 1)),
            dma((layers, tp - 1)),
            dma((layers, tp - 1)),
        ],
        compiler_params=pltpu.CompilerParams(
            collective_id=0, has_side_effects=True, vmem_limit_bytes=67043328
        ),
    )(
        lengths,
        tokens,
        in_gain,
        decay_base,
        mix_gain,
        w_recept,
        w_key,
        w_value,
        w_decay,
        w_rate,
        w_gate,
        w_out,
        states,
    )


def solution(mesh):
    in_specs = (
        P("tp", "dp"),
        P("dp"),
        P(None, "dp"),
        P(None, "dp", "tp"),
        P(None, "dp", "tp"),
        P(None, "dp", "tp"),
        P(None, "dp", "tp"),
        P(None, "dp", "tp"),
        P(None, "dp", "tp"),
        P(None, "tp", "dp"),
        P(None, "tp"),
        P(None, "tp"),
        P(None, "dp", "tp", None, None),
    )
    out_specs = (P("tp", "dp"), P(None, "dp", "tp", None, None))
    return jax.shard_map(
        on_device, mesh=mesh, in_specs=in_specs, out_specs=out_specs, check_vma=False
    )
```

profile of v0, /device:TPU:0, one launch (start us, length us, event | category | flops | bytes accessed | tf_op | source)
XLA Modules:
  0.0 46.0 jit_solution(13575036992250653793)
XLA Ops:
  0.6 40.9 %shard_map.140 = (bf16[4,1024]{1,0:T(4,128)(2,1)}, f32[2,8,4,64,64]{4,3,2,1,0:T(8,128)}) custom-call(s32[8]{0:T(128)} %lengths_hbm.1, bf16[4,1024]{1,0:T(4,128)(2,1)} %tokens.1, f32[2,1024]{1,0:T(2,128)} %in_gain.1, f32[2,256]{1,0:T(2,128)} %decay_base.1, f32[2,256]{1,0:T(2,128)} %mix_gain.1, bf16[2,1024,256]{2,1,0:T(8,128)(2,1)} %w_recept.1, ...), custom_call_target="tpu_custom_call" | custom-call | tf_op jit(solution)/shard_map/pallas_call | solution.py:291
  41.6 1.3 %copy.17 = bf16[4,1024]{1,0:T(4,128)(2,1)} copy(bf16[4,1024]{1,0:T(4,128)(2,1)} %get-tuple-element.4) | data formatting | bytes 16384
  42.9 3.2 %copy.18 = f32[2,8,4,64,64]{4,3,2,1,0:T(8,128)} copy(f32[2,8,4,64,64]{4,3,2,1,0:T(8,128)} %get-tuple-element.5) | data formatting | bytes 2097152
where the time goes:
time: 46.2 us; the launch traced here: 46 us
  Pallas kernels  40.9 us (89%)
  local copies, waits for them, and re-layouts  4.46 us (10%)
  between operations  0.64 us (1%)
    pallas_call x1, Pallas kernels, on_device(): pl.pallas_call(functools.partial(step_kernel, tp, dp), out_shape=(jax.Sha...  40.9 us
    unnamed x2, local copies, waits for them, and re-layouts  4.46 us

commit v1 on v0

--- a/solution.py
+++ b/solution.py
@@ -41,7 +41,6 @@
     mixgain_v,
     w_v,
     wo_v,
-    s_v,
     xg,
     x32,
     psum,
@@ -55,7 +54,6 @@
     w_sem,
     wo_sem,
     s_sem,
-    out_sem,
     ag_s,
     ag_r,
     rs_s,
@@ -65,6 +63,7 @@
     os_s,
     os_r,
 ):
+    s_v = new_states
     layers, row_count, heads, size, _ = states.shape
     rt, cl = tokens.shape
     width = heads * size
@@ -137,7 +136,6 @@
     live_rows = len_rows > POSITION
     cube = (heads, size, size)
     eye = lax.broadcasted_iota(jnp.int32, cube, 1) == lax.broadcasted_iota(jnp.int32, cube, 2)
-    out_copies = []
 
     for l in range(layers):
         for copy in incoming:
@@ -233,8 +231,6 @@
             return carry
 
         lax.fori_loop(0, row_count, renew, 0, unroll=True)
-        out_copies.append(pltpu.make_async_copy(s_v.at[l], new_states.at[l], out_sem.at[l]))
-        out_copies[l].start()
 
         wo_copies[l].wait()
         for copy in incoming:
@@ -260,7 +256,16 @@
 
     for copy in sends:
         copy.wait_send()
-    for copy in out_copies:
+
+
+def store_kernel(rows, held, next_tokens, new_states, sem):
+    copies = [
+        pltpu.make_async_copy(held, new_states, sem.at[0]),
+        pltpu.make_async_copy(rows, next_tokens, sem.at[1]),
+    ]
+    for copy in copies:
+        copy.start()
+    for copy in copies:
         copy.wait()
 
 
@@ -286,16 +291,17 @@
     width = heads * size
     batch = rt * tp
     f32, bf16 = jnp.float32, jnp.bfloat16
-    hbm = pl.BlockSpec(memory_space=pl.ANY)
+    hbm = pl.BlockSpec(memory_space=pltpu.HBM)
+    vmem = pl.BlockSpec(memory_space=pltpu.VMEM)
     dma = pltpu.SemaphoreType.DMA
-    return pl.pallas_call(
+    held = pl.pallas_call(
         functools.partial(step_kernel, tp, dp),
         out_shape=(
-            jax.ShapeDtypeStruct(tokens.shape, tokens.dtype),
-            jax.ShapeDtypeStruct(states.shape, states.dtype),
+            pltpu.VMEM(tokens.shape, tokens.dtype),
+            pltpu.VMEM(states.shape, states.dtype),
         ),
         in_specs=[hbm] * 13,
-        out_specs=(pl.BlockSpec(memory_space=pltpu.VMEM), hbm),
+        out_specs=(vmem, vmem),
         scratch_shapes=[
             pltpu.SMEM(lengths.shape, jnp.int32),
             pltpu.VMEM(in_gain.shape, f32),
@@ -303,7 +309,6 @@
             pltpu.VMEM(mix_gain.shape, f32),
             pltpu.VMEM((layers, ROLES) + w_key.shape[1:], bf16),
             pltpu.VMEM(w_out.shape, bf16),
-            pltpu.VMEM(states.shape, f32),
             pltpu.VMEM((layers, tp, rt, cl), bf16),
             pltpu.VMEM((batch, cl), f32),
             pltpu.VMEM((layers, dp, ROLES + 2, row_count, width), bf16),
@@ -317,7 +322,6 @@
             dma((layers, ROLES)),
             dma((layers,)),
             dma((layers,)),
-            dma((layers,)),
             dma((layers, tp - 1)),
             dma((layers, tp - 1)),
             dma((layers, GROUPS, dp - 1)),
@@ -328,9 +332,9 @@
             dma((layers, tp - 1)),
         ],
         compiler_params=pltpu.CompilerParams(
-            collective_id=0, has_side_effects=True, vmem_limit_bytes=67043328
+            collective_id=0, has_side_effects=True, vmem_limit_bytes=25165824
         ),
-    )(
+    )(*[pltpu.with_memory_space_constraint(x, pltpu.HBM) for x in (
         lengths,
         tokens,
         in_gain,
@@ -344,7 +348,18 @@
         w_gate,
         w_out,
         states,
-    )
+    )])
+    return pl.pallas_call(
+        store_kernel,
+        out_shape=(
+            jax.ShapeDtypeStruct(tokens.shape, tokens.dtype),
+            jax.ShapeDtypeStruct(states.shape, states.dtype),
+        ),
+        in_specs=[vmem, vmem],
+        out_specs=(hbm, hbm),
+        scratch_shapes=[dma((2,))],
+        compiler_params=pltpu.CompilerParams(vmem_limit_bytes=1048576),
+    )(*[pltpu.with_memory_space_constraint(x, pltpu.VMEM) for x in held])
 
 
 def solution(mesh):

time: 46.2 us -> 42.5 us (0.920)
  local copies, waits for them, and re-layouts: 4.46 us -> 0 us
  Pallas kernels: 40.9 us -> 41.7 us
    unnamed x2 -> x0, local copies, waits for them, and re-layouts: 4.46 us -> none
    pallas_call x1 -> x2, Pallas kernels: 40.9 us -> 41.7 us  [the longest x1 40.3 us: on_device(): pl.pallas_call(functools.partial(step_kernel, tp, dp), out_shape=(pltpu.V...]
where the time goes in v1:
time: 42.5 us; the launch traced here: 42.3 us
  Pallas kernels  41.7 us (98%)
  between operations  0.64 us (2%)
    pallas_call x1, Pallas kernels, on_device(): pl.pallas_call(functools.partial(step_kernel, tp, dp), out_shape=(pltpu.V...  40.3 us
    pallas_call x1, Pallas kernels, on_device(): pl.pallas_call(store_kernel, out_shape=(jax.ShapeDtypeStruct(tokens.shape...  1.34 us

profile of v1, /device:TPU:0, one launch (start us, length us, event | category | flops | bytes accessed | tf_op | source)
XLA Modules:
  0.0 42.3 jit_solution(8265600370109537326)
XLA Ops:
  0.6 40.3 %shard_map.140 = (bf16[4,1024]{1,0:T(4,128)(2,1)S(1)}, f32[2,8,4,64,64]{4,3,2,1,0:T(8,128)S(1)}) custom-call(s32[8]{0:T(128)} %lengths_hbm.1, bf16[4,1024]{1,0:T(4,128)(2,1)} %tokens.1, f32[2,1024]{1,0:T(2,128)} %in_gain.1, f32[2,256]{1,0:T(2,128)} %decay_base.1, f32[2,256]{1,0:T(2,128)} %mix_gain.1, bf16[2,1024,256]{2,1,0:T(8,128)(2,1)} %w_recept.1, ...), custom_call_target="tpu_custom_call" | custom-call | tf_op jit(solution)/shard_map/pallas_call | solution.py:297
  41.0 1.3 %shard_map.141 = (bf16[4,1024]{1,0:T(4,128)(2,1)}, f32[2,8,4,64,64]{4,3,2,1,0:T(8,128)}) custom-call(bf16[4,1024]{1,0:T(4,128)(2,1)S(1)} %get-tuple-element.4.rows, f32[2,8,4,64,64]{4,3,2,1,0:T(8,128)S(1)} %get-tuple-element.5.held), custom_call_target="tpu_custom_call" | custom-call | tf_op jit(solution)/shard_map/pallas_call | solution.py:352
